TPU v7x, 32 devices: a whole 2x2x4 slice. The times are simulated.
32 devices in a mesh: sp: 16 (over z, y, core), tp: 2 (over x).
Axes of the slice: x: 2, y: 2, z: 4, core: 2. Of those that a mesh axis runs over, the one named last changes fastest.
Arguments:
- query_rows: bfloat16 [8192, 1024], P(('sp', 'tp')), may hold values from -6 to 6
- key_rows: bfloat16 [8192, 1024], P(('sp', 'tp')), may hold values from -6 to 6
- value_rows: bfloat16 [8192, 1024], P(('sp', 'tp')), may hold values from -6 to 6
- out_grad: bfloat16 [8192, 1024], P(('sp', 'tp')), may hold values from -40 to 40
- log_totals: float32 [8192, 8], P(('sp', 'tp')), may hold values from 6 to 7.5
- out_dot: float32 [8192, 8], P(('sp', 'tp')), may hold values from -6 to 6
- bias_table: float32 [8, 320], replicated, may hold values from -4 to 4
Outputs:
- grad_query: bfloat16 [8192, 1024], P(('sp', 'tp'))
- grad_key: bfloat16 [8192, 1024], P(('sp', 'tp'))
- grad_value: bfloat16 [8192, 1024], P(('sp', 'tp'))
- grad_table: float32 [8, 320], replicated
All inputs are finite; a program needn't handle non-finite values.
Results may differ from a plain program's by a relative error of at most 0.005.
Values may be sent and summed in bfloat16 or wider, within the bound.
A program may use at most 128 MiB of HBM per device.

v0:
```python
import functools
import math

import jax
import jax.numpy as jnp
from jax import lax
from jax.experimental import pallas as pl
from jax.experimental.pallas import tpu as pltpu
from jax.sharding import PartitionSpec as P

SEG_LEN = 64
LEFT_SEGS = 8
REL_CLIP = 256
LANES = 128
SUBL = 8
MASKED = -1e30
LOG2E = math.log2(math.e)
MESH = pl.DeviceIdType.MESH


def axis_stages(size):
    stages, stride = [], 1
    while size > 1:
        factor = next((f for f in (8, 4, 3, 2, 5, 7) if size % f == 0), size)
        stages.append((stride, factor))
        stride *= factor
        size //= factor
    return stages


def iota(shape, axis):
    return lax.broadcasted_iota(jnp.int32, shape, axis)


def turn(x, amount):
    width = x.shape[1]
    return pltpu.roll(x, amount % width, 1)


def fold_diagonals(x):
    rows = x.shape[0]
    while rows > SUBL:
        half = rows // 2
        x = x[:half] + turn(x[half:], -half)
        rows = half
    return x


def fold_rows(x):
    rows = x.shape[0]
    while rows > SUBL:
        half = rows // 2
        x = x[:half] + x[half:]
        rows = half
    return x


def sublane_turn(x, direction):
    subl = iota(x.shape, 0)
    for bit in (1, 2, 4):
        x = jnp.where((subl & bit) != 0, turn(x, direction * bit), x)
    return x


def kernel(
    sizes,
    q_hbm, k_hbm, v_hbm, g_hbm, log_hbm, dot_hbm, table_hbm,
    dq_ref, dk_ref, dv_ref, dt_ref,
    q_ref, g_ref, k_ref, v_ref, log_ref, dot_ref, table_ref, load_sem,
    stat, stat_in, qg_in, part_out, part_in, dq_own, dk_acc, dv_acc,
    bias, edge, tab, neg, const, acc_pos, acc_neg, acc_const, tab_slots,
    stat_send, stat_recv, qg_send, qg_recv, part_send, part_recv, tab_send, tab_recv,
):
    sp_size, tp_size = sizes
    total = sp_size * tp_size
    rows, features = q_ref.shape
    heads, table_len = table_ref.shape
    head_dim = features // heads
    inv_root = head_dim ** -0.5
    table_width = tab.shape[1]
    sp, tp = lax.axis_index("sp"), lax.axis_index("tp")
    me = sp * tp_size + tp

    def device(index):
        return (index // tp_size, lax.rem(index, tp_size))

    stages = axis_stages(total)[::-1]

    def stage_place(stage):
        stride, factor = stage
        return lax.rem(me // stride, factor)

    def stage_peer(stage, place):
        return device(me + (place - stage_place(stage)) * stage[0])

    loads = [
        pltpu.make_async_copy(source, target, load_sem.at[at])
        for at, (source, target) in enumerate((
            (q_hbm, q_ref), (g_hbm, g_ref), (log_hbm, log_ref), (dot_hbm, dot_ref),
            (table_hbm, table_ref), (k_hbm, k_ref), (v_hbm, v_ref),
        ))
    ]
    for load in loads:
        load.start()

    barrier = pltpu.get_barrier_semaphore()
    count = 0
    for lag in (1, 2):
        for other in (me + lag, me - lag):
            valid = (other >= 0) & (other < total)
            count = count + jnp.where(valid, 1, 0)

            @pl.when(valid)
            def _():
                pl.semaphore_signal(barrier, inc=1, device_id=device(other), device_id_type=MESH)

    for stage in stages:
        for offset in range(1, stage[1]):
            place = lax.rem(stage_place(stage) + offset, stage[1])
            pl.semaphore_signal(
                barrier, inc=1, device_id=stage_peer(stage, place), device_id_type=MESH
            )
            count = count + 1

    for load in loads[:4]:
        load.wait()
    stat[0:heads, :] = log_ref[...] * LOG2E
    stat[heads:, :] = dot_ref[...]
    pl.semaphore_wait(barrier, count)

    def columns(head):
        return pl.ds(pl.multiple_of(head * head_dim, head_dim), head_dim)

    def stat_copy(lag):
        return pltpu.make_async_remote_copy(
            src_ref=stat, dst_ref=stat_in.at[lag - 1],
            send_sem=stat_send.at[lag - 1], recv_sem=stat_recv.at[lag - 1],
            device_id=device(me - lag), device_id_type=MESH,
        )

    def qg_copy(lag, which, head):
        return pltpu.make_async_remote_copy(
            src_ref=(q_ref, g_ref)[which].at[:, columns(head)],
            dst_ref=qg_in.at[lag - 1, which, head],
            send_sem=qg_send.at[lag - 1, which, head], recv_sem=qg_recv.at[lag - 1, which, head],
            device_id=device(me - lag), device_id_type=MESH,
        )

    def part_copy(lag, head):
        return pltpu.make_async_remote_copy(
            src_ref=part_out.at[lag - 1, head], dst_ref=part_in.at[lag - 1, head],
            send_sem=part_send.at[lag - 1, head], recv_sem=part_recv.at[lag - 1, head],
            device_id=device(me + lag), device_id_type=MESH,
        )

    for lag in (1, 2):
        @pl.when(me >= lag)
        def _():
            stat_copy(lag).start()

    @pl.loop(0, heads)
    def _(head):
        for lag in (1, 2):
            @pl.when(me >= lag)
            def _():
                qg_copy(lag, 0, head).start()
                qg_copy(lag, 1, head).start()

    loads[4].wait()
    tab[...] = jnp.zeros_like(tab)
    tab[:, 0:table_len] = table_ref[...] * LOG2E
    padded = tab[...]
    from_zero = turn(padded, 1 - SEG_LEN)
    neg[...] = turn(padded, LANES - (SEG_LEN - 1))[:, 0:LANES]
    const[...] = jnp.broadcast_to(from_zero[:, rows:rows + 1], const.shape)
    tab[...] = from_zero
    key_at, query_at = iota((rows, rows), 0), iota((rows, rows), 1)
    edge[...] = jnp.where(query_at // SEG_LEN <= key_at // SEG_LEN, 0.0, MASKED)

    @pl.loop(0, heads)
    def _(head):
        row = jnp.broadcast_to(tab[pl.ds(head, 1), 0:rows], (SUBL, rows))
        near = sublane_turn(row, 1)
        row = jnp.broadcast_to(neg[pl.ds(head, 1), :], (SUBL, LANES))
        before = sublane_turn(row, 1)
        have = SUBL
        while have < rows:
            near = jnp.concatenate([near, turn(near, have)], axis=0)
            if have < LANES:
                before = jnp.concatenate([before, turn(before, have)], axis=0)
            have *= 2
        far = const[pl.ds(head, 1), :]
        upper = iota((rows, rows), 1) >= iota((rows, rows), 0)
        bias[1, head] = jnp.where(upper, far, near)
        segs_ok = iota((rows, rows), 1) // SEG_LEN >= iota((rows, rows), 0) // SEG_LEN
        wide = jnp.concatenate([before] * (rows // LANES), axis=1)
        tall = jnp.concatenate([wide] * (rows // LANES), axis=0)
        bias[0, head] = jnp.where(upper, near, jnp.where(segs_ok, tall, MASKED))

    def pair_terms(lag, head, queries, grads, log_row, dot_row):
        keys, values = k_ref[:, columns(head)], v_ref[:, columns(head)]
        across = (((1,), (1,)), ((), ()))
        scores = lax.dot_general(keys, queries, across, preferred_element_type=jnp.float32)
        if lag < 2:
            shift = bias[lag, head] - log_row
        else:
            shift = edge[...] + (const[pl.ds(head, 1), :] - log_row)
        weights = jnp.exp2(scores * (inv_root * LOG2E) + shift)
        weight_grads = lax.dot_general(values, grads, across, preferred_element_type=jnp.float32)
        score_grads = weights * (weight_grads - dot_row)
        score_grads_b = score_grads.astype(jnp.bfloat16)
        value_part = jnp.dot(
            weights.astype(jnp.bfloat16), grads, preferred_element_type=jnp.float32
        )
        key_part = jnp.dot(score_grads_b, queries, preferred_element_type=jnp.float32)
        query_part = lax.dot_general(
            score_grads_b, keys, (((0,), (0,)), ((), ())), preferred_element_type=jnp.float32
        )
        return score_grads, query_part, key_part, value_part

    loads[5].wait()
    loads[6].wait()

    @pl.loop(0, heads)
    def _(head):
        score_grads, query_part, key_part, value_part = pair_terms(
            0, head, q_ref[:, columns(head)], g_ref[:, columns(head)],
            stat[pl.ds(head, 1), :], stat[pl.ds(head + heads, 1), :],
        )
        dq_own[head] = query_part
        dk_acc[head] = key_part
        dv_acc[head] = value_part
        upper = iota((rows, rows), 1) >= iota((rows, rows), 0)
        acc_pos[head] = fold_diagonals(jnp.where(upper, score_grads, 0.0))
        lower = jnp.where(upper, 0.0, score_grads)
        tiles = sum(
            lower[at:at + LANES, at:at + LANES] for at in range(0, rows, LANES)
        )
        acc_neg[head] = fold_diagonals(tiles)
        acc_const[head] = jnp.zeros(acc_const.shape[1:], jnp.float32)

    for lag in (2, 1):
        @pl.when(me + lag < total)
        def _():
            stat_copy(lag).wait_recv()

    @pl.loop(0, heads)
    def _(head):
        for lag in (2, 1):
            @pl.when(me + lag < total)
            def _():
                qg_copy(lag, 0, head).wait_recv()
                qg_copy(lag, 1, head).wait_recv()
                score_grads, query_part, key_part, value_part = pair_terms(
                    lag, head, qg_in[lag - 1, 0, head], qg_in[lag - 1, 1, head],
                    stat_in[lag - 1, pl.ds(head, 1), :],
                    stat_in[lag - 1, pl.ds(head + heads, 1), :],
                )
                part_out[lag - 1, head] = query_part.astype(jnp.bfloat16)
                part_copy(lag, head).start()
                dk_acc[head] += key_part
                dv_acc[head] += value_part
                if lag == 1:
                    upper = iota((rows, rows), 1) >= iota((rows, rows), 0)
                    acc_const[head] += fold_rows(jnp.where(upper, score_grads, 0.0))
                    acc_pos[head] += fold_diagonals(jnp.where(upper, 0.0, score_grads))
                else:
                    acc_const[head] += fold_rows(score_grads)

        dk_ref[:, columns(head)] = (dk_acc[head] * inv_root).astype(dk_ref.dtype)
        dv_ref[:, columns(head)] = dv_acc[head].astype(dv_ref.dtype)
        near = jnp.sum(sublane_turn(acc_pos[head], -1), axis=0, keepdims=True)
        before = jnp.sum(sublane_turn(acc_neg[head], -1), axis=0, keepdims=True)
        far = jnp.sum(jnp.sum(acc_const[head], axis=0, keepdims=True), axis=1, keepdims=True)
        tail = jnp.broadcast_to(far, (1, table_width - rows))
        tail = jnp.where(iota(tail.shape, 1) == 0, tail, 0.0)
        here = iota(tab.shape, 0) == head
        tab[...] = jnp.where(here, jnp.concatenate([near, tail], axis=1), tab[...])
        neg[...] = jnp.where(iota(neg.shape, 0) == head, before, neg[...])

    spread = jnp.concatenate(
        [neg[...], jnp.zeros((heads, table_width - LANES), jnp.float32)], axis=1
    )
    running = turn(tab[...], SEG_LEN - 1) + turn(spread, -(LANES - (SEG_LEN - 1)))

    def tab_copy(at, place, peer_place):
        stage = stages[at]
        return pltpu.make_async_remote_copy(
            src_ref=tab_slots.at[at, place], dst_ref=tab_slots.at[at, place],
            send_sem=tab_send.at[at, peer_place], recv_sem=tab_recv.at[at, place],
            device_id=stage_peer(stage, peer_place), device_id_type=MESH,
        )

    def stage_start(at, block):
        place = stage_place(stages[at])
        tab_slots[at, place] = block
        for offset in range(1, stages[at][1]):
            tab_copy(at, place, lax.rem(place + offset, stages[at][1])).start()

    def stage_finish(at):
        factor = stages[at][1]
        place = stage_place(stages[at])
        for offset in range(1, factor):
            other = lax.rem(place + offset, factor)
            tab_copy(at, other, other).wait_recv()
        out = tab_slots[at, 0]
        for member in range(1, factor):
            out = out + tab_slots[at, member]
        return out

    def finish_queries(first, last):
        @pl.loop(first, last)
        def _(head):
            for lag in (2, 1):
                @pl.when(me >= lag)
                def _():
                    part_copy(lag, head).wait_recv()
                    dq_own[head] += part_in[lag - 1, head].astype(jnp.float32)
            dq_ref[:, columns(head)] = (dq_own[head] * inv_root).astype(dq_ref.dtype)

    if stages:
        stage_start(0, running)
    for at in range(len(stages)):
        finish_queries(heads * at // (2 * len(stages)), heads * (at + 1) // (2 * len(stages)))
        running = stage_finish(at)
        if at + 1 < len(stages):
            stage_start(at + 1, running)
    finish_queries(heads // 2 if stages else 0, heads)
    dt_ref[...] = running[:, 0:table_len]

    for lag in (1, 2):
        @pl.when(me >= lag)
        def _():
            stat_copy(lag).wait_send()

    @pl.loop(0, heads)
    def _(head):
        for lag in (1, 2):
            @pl.when(me >= lag)
            def _():
                qg_copy(lag, 0, head).wait_send()
                qg_copy(lag, 1, head).wait_send()

            @pl.when(me + lag < total)
            def _():
                part_copy(lag, head).wait_send()

    for at, stage in enumerate(stages):
        place = stage_place(stage)
        for offset in range(1, stage[1]):
            tab_copy(at, place, lax.rem(place + offset, stage[1])).wait_send()


def store_kernel(*refs):
    sources, targets, held, in_sem, out_sem = refs[:4], refs[4:8], refs[8:12], refs[12], refs[13]
    loads = [pltpu.make_async_copy(sources[at], held[at], in_sem.at[at]) for at in range(4)]
    stores = [pltpu.make_async_copy(held[at], targets[at], out_sem.at[at]) for at in range(4)]
    for load in loads:
        load.start()
    for load, store in zip(loads, stores):
        load.wait()
        store.start()
    for store in stores:
        store.wait()


def local(sizes, query_rows, key_rows, value_rows, out_grad, log_totals, out_dot, bias_table):
    rows, features = query_rows.shape
    heads, table_len = bias_table.shape
    head_dim = features // heads
    assert LEFT_SEGS * SEG_LEN == 2 * rows and rows == REL_CLIP
    assert table_len == REL_CLIP + SEG_LEN and head_dim == LANES
    stage_list = axis_stages(sizes[0] * sizes[1])
    stage_count = max(len(stage_list), 1)
    slot_count = max([factor for _, factor in stage_list] + [1])
    table_width = -(-(table_len + 1) // LANES) * LANES
    f32, bf16 = jnp.float32, jnp.bfloat16
    vmem = pl.BlockSpec(memory_space=pltpu.VMEM)
    dma = pltpu.SemaphoreType.DMA
    wide = jax.ShapeDtypeStruct((rows, features), bf16)
    results = pl.pallas_call(
        functools.partial(kernel, sizes),
        out_shape=(wide, wide, wide, jax.ShapeDtypeStruct((heads, table_len), f32)),
        in_specs=[pl.BlockSpec(memory_space=pltpu.HBM)] * 7,
        out_specs=(vmem,) * 4,
        scratch_shapes=[
            pltpu.VMEM((rows, features), bf16),
            pltpu.VMEM((rows, features), bf16),
            pltpu.VMEM((rows, features), bf16),
            pltpu.VMEM((rows, features), bf16),
            pltpu.VMEM((heads, rows), f32),
            pltpu.VMEM((heads, rows), f32),
            pltpu.VMEM((heads, table_len), f32),
            dma((7,)),
            pltpu.VMEM((2 * heads, rows), f32),
            pltpu.VMEM((2, 2 * heads, rows), f32),
            pltpu.VMEM((2, 2, heads, rows, head_dim), bf16),
            pltpu.VMEM((2, heads, rows, head_dim), bf16),
            pltpu.VMEM((2, heads, rows, head_dim), bf16),
            pltpu.VMEM((heads, rows, head_dim), f32),
            pltpu.VMEM((heads, rows, head_dim), f32),
            pltpu.VMEM((heads, rows, head_dim), f32),
            pltpu.VMEM((2, heads, rows, rows), f32),
            pltpu.VMEM((rows, rows), f32),
            pltpu.VMEM((heads, table_width), f32),
            pltpu.VMEM((heads, LANES), f32),
            pltpu.VMEM((heads, rows), f32),
            pltpu.VMEM((heads, SUBL, rows), f32),
            pltpu.VMEM((heads, SUBL, LANES), f32),
            pltpu.VMEM((heads, SUBL, rows), f32),
            pltpu.VMEM((stage_count, slot_count, heads, table_width), f32),
            dma((2,)), dma((2,)),
            dma((2, 2, heads)), dma((2, 2, heads)),
            dma((2, heads)), dma((2, heads)),
            dma((stage_count, slot_count)), dma((stage_count, slot_count)),
        ],
        compiler_params=pltpu.CompilerParams(
            collective_id=0, has_side_effects=True, vmem_limit_bytes=67043328
        ),
        name="band_backward",
    )(query_rows, key_rows, value_rows, out_grad, log_totals.T, out_dot.T, bias_table)
    return pl.pallas_call(
        store_kernel,
        out_shape=tuple(jax.ShapeDtypeStruct(x.shape, x.dtype) for x in results),
        in_specs=[pl.BlockSpec(memory_space=pltpu.HBM)] * 4,
        out_specs=(pl.BlockSpec(memory_space=pltpu.HBM),) * 4,
        scratch_shapes=[pltpu.VMEM(x.shape, x.dtype) for x in results] + [dma((4,)), dma((4,))],
        compiler_params=pltpu.CompilerParams(vmem_limit_bytes=67043328),
        name="store",
    )(*results)


def solution(mesh):
    sizes = (mesh.shape["sp"], mesh.shape["tp"])
    by_rows = P(("sp", "tp"), None)
    return jax.shard_map(
        functools.partial(local, sizes),
        mesh=mesh,
        in_specs=(by_rows,) * 6 + (P(),),
        out_specs=(by_rows, by_rows, by_rows, P()),
        check_vma=False,
    )
```

profile of v0, /device:TPU:0, one launch (start us, length us, event | category | flops | bytes accessed | tf_op | source)
XLA Modules:
  0.0 48.4 jit_solution(2462110881600459038)
XLA Ops:
  0.6 45.5 %band_backward.1 = (bf16[256,1024]{1,0:T(8,128)(2,1)}, bf16[256,1024]{1,0:T(8,128)(2,1)}, bf16[256,1024]{1,0:T(8,128)(2,1)}, f32[8,320]{1,0:T(8,128)}) custom-call(bf16[256,1024]{1,0:T(8,128)(2,1)} %q_hbm.1, bf16[256,1024]{1,0:T(8,128)(2,1)} %k_hbm.1, bf16[256,1024]{1,0:T(8,128)(2,1)} %v_hbm.1, bf16[256,1024]{1,0:T(8,128)(2,1)} %g_hbm.1, f32[8,256]{1,0:T(8,128)} %bitcast.2, ...), custom_call_target="tpu_custom_call" | custom-call | tf_op jit(solution)/shard_map/band_backward/pallas_call | solution.py:381
  46.2 2.3 %store.1 = (bf16[256,1024]{1,0:T(8,128)(2,1)}, bf16[256,1024]{1,0:T(8,128)(2,1)}, bf16[256,1024]{1,0:T(8,128)(2,1)}, f32[8,320]{1,0:T(8,128)}) custom-call(bf16[256,1024]{1,0:T(8,128)(2,1)} %get-tuple-element.8.refs_0_, bf16[256,1024]{1,0:T(8,128)(2,1)} %get-tuple-element.9.refs_1_, bf16[256,1024]{1,0:T(8,128)(2,1)} %get-tuple-element.10.refs_2_, ...), custom_call_target="tpu_custom_call" | custom-call | tf_op jit(solution)/shard_map/store/pallas_call | solution.py:422
where the time goes:
time: 48.6 us; the launch traced here: 48.4 us
  Pallas kernels  47.8 us (98%)
  between operations  0.64 us (1%)
    pallas_call x1, Pallas kernels, local(): pl.pallas_call(functools.partial(kernel, sizes), out_shape=(wide, wide, w...  45.5 us
    pallas_call x1, Pallas kernels, local(): pl.pallas_call(store_kernel, out_shape=tuple((jax.ShapeDtypeStruct(x.shap...  2.25 us

commit v1 on v0

--- a/solution.py
+++ b/solution.py
@@ -21,7 +21,8 @@
 def axis_stages(size):
     stages, stride = [], 1
     while size > 1:
-        factor = next((f for f in (8, 4, 3, 2, 5, 7) if size % f == 0), size)
+        order = (8, 4, 3, 2, 5, 7) if stages else (4, 3, 2, 5, 7)
+        factor = next((f for f in order if size % f == 0), size)
         stages.append((stride, factor))
         stride *= factor
         size //= factor
@@ -70,6 +71,7 @@
     stat, stat_in, qg_in, part_out, part_in, dq_own, dk_acc, dv_acc,
     bias, edge, tab, neg, const, acc_pos, acc_neg, acc_const, tab_slots,
     stat_send, stat_recv, qg_send, qg_recv, part_send, part_recv, tab_send, tab_recv,
+    qg_load, flood_sem, relay_send,
 ):
     sp_size, tp_size = sizes
     total = sp_size * tp_size
@@ -86,6 +88,11 @@
 
     stages = axis_stages(total)[::-1]
 
+    group = stages[-1][1] if stages else 1
+    inside = lax.rem(me + 1, group) != 0
+    sends = [None, (me >= 1) & (lax.rem(me, group) != 0), me >= 2]
+    relays = (me + 2 < total) & (lax.rem(me + 2, group) == 0)
+
     def stage_place(stage):
         stride, factor = stage
         return lax.rem(me // stride, factor)
@@ -93,14 +100,28 @@
     def stage_peer(stage, place):
         return device(me + (place - stage_place(stage)) * stage[0])
 
+    def columns(head):
+        return pl.ds(pl.multiple_of(head * head_dim, head_dim), head_dim)
+
+    def qg_load_copy(which, head):
+        return pltpu.make_async_copy(
+            (q_hbm, g_hbm)[which].at[:, columns(head)], (q_ref, g_ref)[which].at[:, columns(head)],
+            qg_load.at[which, head],
+        )
+
+    def start_qg_loads(head):
+        qg_load_copy(0, head).start()
+        qg_load_copy(1, head).start()
+
     loads = [
         pltpu.make_async_copy(source, target, load_sem.at[at])
         for at, (source, target) in enumerate((
-            (q_hbm, q_ref), (g_hbm, g_ref), (log_hbm, log_ref), (dot_hbm, dot_ref),
+            (log_hbm, log_ref), (dot_hbm, dot_ref),
             (table_hbm, table_ref), (k_hbm, k_ref), (v_hbm, v_ref),
         ))
     ]
-    for load in loads:
+    start_qg_loads(0)
+    for load in loads[:2]:
         load.start()
 
     barrier = pltpu.get_barrier_semaphore()
@@ -114,22 +135,10 @@
             def _():
                 pl.semaphore_signal(barrier, inc=1, device_id=device(other), device_id_type=MESH)
 
-    for stage in stages:
-        for offset in range(1, stage[1]):
-            place = lax.rem(stage_place(stage) + offset, stage[1])
-            pl.semaphore_signal(
-                barrier, inc=1, device_id=stage_peer(stage, place), device_id_type=MESH
-            )
-            count = count + 1
-
-    for load in loads[:4]:
-        load.wait()
-    stat[0:heads, :] = log_ref[...] * LOG2E
-    stat[heads:, :] = dot_ref[...]
+    pl.loop(1, heads)(start_qg_loads)
+    for load in loads[2:]:
+        load.start()
     pl.semaphore_wait(barrier, count)
-
-    def columns(head):
-        return pl.ds(pl.multiple_of(head * head_dim, head_dim), head_dim)
 
     def stat_copy(lag):
         return pltpu.make_async_remote_copy(
@@ -146,6 +155,18 @@
             device_id=device(me - lag), device_id_type=MESH,
         )
 
+    def relay_copy(which, head):
+        return pltpu.make_async_remote_copy(
+            src_ref=qg_in.at[1, which, head], dst_ref=qg_in.at[0, which, head],
+            send_sem=relay_send.at[which, head], recv_sem=qg_recv.at[0, which, head],
+            device_id=device(me + 1), device_id_type=MESH,
+        )
+
+    def relay(head):
+        for which in (0, 1):
+            qg_copy(2, which, head).wait_recv()
+            relay_copy(which, head).start()
+
     def part_copy(lag, head):
         return pltpu.make_async_remote_copy(
             src_ref=part_out.at[lag - 1, head], dst_ref=part_in.at[lag - 1, head],
@@ -153,20 +174,54 @@
             device_id=device(me + lag), device_id_type=MESH,
         )
 
-    for lag in (1, 2):
-        @pl.when(me >= lag)
-        def _():
-            stat_copy(lag).start()
-
-    @pl.loop(0, heads)
-    def _(head):
+    def send_qg(head):
+        qg_load_copy(0, head).wait()
+        qg_load_copy(1, head).wait()
         for lag in (1, 2):
-            @pl.when(me >= lag)
+            @pl.when(sends[lag])
             def _():
                 qg_copy(lag, 0, head).start()
                 qg_copy(lag, 1, head).start()
 
-    loads[4].wait()
+    send_qg(0)
+    for load in loads[:2]:
+        load.wait()
+    stat[0:heads, :] = log_ref[...] * LOG2E
+    stat[heads:, :] = dot_ref[...]
+    for lag in (1, 2):
+        @pl.when(me >= lag)
+        def _():
+            stat_copy(lag).start()
+
+    pl.loop(1, heads)(send_qg)
+
+    reaches, reach = [], 2
+    while reach < max([stride * (factor - 1) for stride, factor in stages] + [0]):
+        reaches.append(reach)
+        reach *= 2
+
+    def flood_others(at):
+        others = (me + reaches[at], me - reaches[at])
+        return [(other, (other >= 0) & (other < total)) for other in others]
+
+    def flood_start(at):
+        if at < len(reaches):
+            for other, valid in flood_others(at):
+                @pl.when(valid)
+                def _():
+                    pl.semaphore_signal(
+                        flood_sem.at[at], inc=1, device_id=device(other), device_id_type=MESH
+                    )
+
+    def flood_finish(at):
+        if at < len(reaches):
+            pl.semaphore_wait(
+                flood_sem.at[at], sum(jnp.where(valid, 1, 0) for _, valid in flood_others(at))
+            )
+
+    flood_start(0)
+
+    loads[2].wait()
     tab[...] = jnp.zeros_like(tab)
     tab[:, 0:table_len] = table_ref[...] * LOG2E
     padded = tab[...]
@@ -218,8 +273,9 @@
         )
         return score_grads, query_part, key_part, value_part
 
-    loads[5].wait()
-    loads[6].wait()
+    loads[3].wait()
+    loads[4].wait()
+    in_loop = min(len(reaches), heads // 2)
 
     @pl.loop(0, heads)
     def _(head):
@@ -238,6 +294,24 @@
         )
         acc_neg[head] = fold_diagonals(tiles)
         acc_const[head] = jnp.zeros(acc_const.shape[1:], jnp.float32)
+        @pl.when(relays & (lax.rem(head, 2) == 1))
+        def _():
+            relay(head // 2)
+
+        for at in range(in_loop):
+            @pl.when(head == 2 * at + 1)
+            def _():
+                flood_finish(at)
+                flood_start(at + 1)
+
+    def start_parts(first, last):
+        @pl.loop(first, last)
+        def _(head):
+            part_copy(1, head).start()
+
+    for at in range(in_loop, len(reaches)):
+        flood_finish(at)
+        flood_start(at + 1)
 
     for lag in (2, 1):
         @pl.when(me + lag < total)
@@ -246,18 +320,26 @@
 
     @pl.loop(0, heads)
     def _(head):
+        @pl.when(relays & (head < heads - heads // 2))
+        def _():
+            relay(head + heads // 2)
+
         for lag in (2, 1):
             @pl.when(me + lag < total)
             def _():
-                qg_copy(lag, 0, head).wait_recv()
-                qg_copy(lag, 1, head).wait_recv()
+                @pl.when((lag == 1) | ~relays)
+                def _():
+                    qg_copy(lag, 0, head).wait_recv()
+                    qg_copy(lag, 1, head).wait_recv()
+
                 score_grads, query_part, key_part, value_part = pair_terms(
                     lag, head, qg_in[lag - 1, 0, head], qg_in[lag - 1, 1, head],
                     stat_in[lag - 1, pl.ds(head, 1), :],
                     stat_in[lag - 1, pl.ds(head + heads, 1), :],
                 )
                 part_out[lag - 1, head] = query_part.astype(jnp.bfloat16)
-                part_copy(lag, head).start()
+                if lag == 2:
+                    part_copy(2, head).start()
                 dk_acc[head] += key_part
                 dv_acc[head] += value_part
                 if lag == 1:
@@ -266,6 +348,10 @@
                     acc_pos[head] += fold_diagonals(jnp.where(upper, 0.0, score_grads))
                 else:
                     acc_const[head] += fold_rows(score_grads)
+
+        @pl.when((me + 1 < total) & inside & (head == heads - 2))
+        def _():
+            start_parts(0, heads - 1)
 
         dk_ref[:, columns(head)] = (dk_acc[head] * inv_root).astype(dk_ref.dtype)
         dv_ref[:, columns(head)] = dv_acc[head].astype(dv_ref.dtype)
@@ -320,12 +406,21 @@
 
     if stages:
         stage_start(0, running)
-    for at in range(len(stages)):
-        finish_queries(heads * at // (2 * len(stages)), heads * (at + 1) // (2 * len(stages)))
-        running = stage_finish(at)
-        if at + 1 < len(stages):
-            stage_start(at + 1, running)
-    finish_queries(heads // 2 if stages else 0, heads)
+
+    @pl.when((me + 1 < total) & ~inside)
+    def _():
+        start_parts(0, heads)
+
+    for at in range(len(stages) - 1):
+        stage_start(at + 1, stage_finish(at))
+
+    @pl.when((me + 1 < total) & inside)
+    def _():
+        start_parts(heads - 1, heads)
+
+    finish_queries(0, heads)
+    if stages:
+        running = stage_finish(len(stages) - 1)
     dt_ref[...] = running[:, 0:table_len]
 
     for lag in (1, 2):
@@ -336,7 +431,7 @@
     @pl.loop(0, heads)
     def _(head):
         for lag in (1, 2):
-            @pl.when(me >= lag)
+            @pl.when(sends[lag])
             def _():
                 qg_copy(lag, 0, head).wait_send()
                 qg_copy(lag, 1, head).wait_send()
@@ -344,6 +439,11 @@
             @pl.when(me + lag < total)
             def _():
                 part_copy(lag, head).wait_send()
+
+        @pl.when(relays)
+        def _():
+            relay_copy(0, head).wait_send()
+            relay_copy(1, head).wait_send()
 
     for at, stage in enumerate(stages):
         place = stage_place(stage)
@@ -352,13 +452,9 @@
 
 
 def store_kernel(*refs):
-    sources, targets, held, in_sem, out_sem = refs[:4], refs[4:8], refs[8:12], refs[12], refs[13]
-    loads = [pltpu.make_async_copy(sources[at], held[at], in_sem.at[at]) for at in range(4)]
-    stores = [pltpu.make_async_copy(held[at], targets[at], out_sem.at[at]) for at in range(4)]
-    for load in loads:
-        load.start()
-    for load, store in zip(loads, stores):
-        load.wait()
+    sources, targets, sem = refs[:4], refs[4:8], refs[8]
+    stores = [pltpu.make_async_copy(sources[at], targets[at], sem.at[at]) for at in range(4)]
+    for store in stores:
         store.start()
     for store in stores:
         store.wait()
@@ -377,10 +473,10 @@
     f32, bf16 = jnp.float32, jnp.bfloat16
     vmem = pl.BlockSpec(memory_space=pltpu.VMEM)
     dma = pltpu.SemaphoreType.DMA
-    wide = jax.ShapeDtypeStruct((rows, features), bf16)
+    wide = pltpu.VMEM((rows, features), bf16)
     results = pl.pallas_call(
         functools.partial(kernel, sizes),
-        out_shape=(wide, wide, wide, jax.ShapeDtypeStruct((heads, table_len), f32)),
+        out_shape=(wide, wide, wide, pltpu.VMEM((heads, table_len), f32)),
         in_specs=[pl.BlockSpec(memory_space=pltpu.HBM)] * 7,
         out_specs=(vmem,) * 4,
         scratch_shapes=[
@@ -391,7 +487,7 @@
             pltpu.VMEM((heads, rows), f32),
             pltpu.VMEM((heads, rows), f32),
             pltpu.VMEM((heads, table_len), f32),
-            dma((7,)),
+            dma((5,)),
             pltpu.VMEM((2 * heads, rows), f32),
             pltpu.VMEM((2, 2 * heads, rows), f32),
             pltpu.VMEM((2, 2, heads, rows, head_dim), bf16),
@@ -413,19 +509,20 @@
             dma((2, 2, heads)), dma((2, 2, heads)),
             dma((2, heads)), dma((2, heads)),
             dma((stage_count, slot_count)), dma((stage_count, slot_count)),
+            dma((2, heads)), pltpu.SemaphoreType.REGULAR((16,)), dma((2, heads)),
         ],
         compiler_params=pltpu.CompilerParams(
-            collective_id=0, has_side_effects=True, vmem_limit_bytes=67043328
+            collective_id=0, has_side_effects=True, vmem_limit_bytes=40 * 2**20
         ),
         name="band_backward",
-    )(query_rows, key_rows, value_rows, out_grad, log_totals.T, out_dot.T, bias_table)
+    )(*(pltpu.with_memory_space_constraint(x, pltpu.HBM) for x in (query_rows, key_rows, value_rows, out_grad, log_totals.T, out_dot.T, bias_table)))
     return pl.pallas_call(
         store_kernel,
         out_shape=tuple(jax.ShapeDtypeStruct(x.shape, x.dtype) for x in results),
-        in_specs=[pl.BlockSpec(memory_space=pltpu.HBM)] * 4,
+        in_specs=[vmem] * 4,
         out_specs=(pl.BlockSpec(memory_space=pltpu.HBM),) * 4,
-        scratch_shapes=[pltpu.VMEM(x.shape, x.dtype) for x in results] + [dma((4,)), dma((4,))],
-        compiler_params=pltpu.CompilerParams(vmem_limit_bytes=67043328),
+        scratch_shapes=[dma((4,))],
+        compiler_params=pltpu.CompilerParams(vmem_limit_bytes=2**20),
         name="store",
     )(*results)
 

time: 48.6 us -> 43.6 us (0.90)
  Pallas kernels: 47.8 us -> 42.8 us
    pallas_call x1, Pallas kernels: 45.5 us -> 41.7 us  [local(): pl.pallas_call(functools.partial(kernel, sizes), out_shape=(wide, wide, w...]
    pallas_call x1, Pallas kernels: 2.25 us -> 1.18 us  [local(): pl.pallas_call(store_kernel, out_shape=tuple((jax.ShapeDtypeStruct(x.shap...]
where the time goes in v1:
time: 43.6 us; the launch traced here: 43.5 us
  Pallas kernels  42.8 us (98%)
  between operations  0.64 us (1%)
    pallas_call x1, Pallas kernels, local(): pl.pallas_call(functools.partial(kernel, sizes), out_shape=(wide, wide, w...  41.7 us
    pallas_call x1, Pallas kernels, local(): pl.pallas_call(store_kernel, out_shape=tuple((jax.ShapeDtypeStruct(x.shap...  1.18 us

profile of v1, /device:TPU:0, one launch (start us, length us, event | category | flops | bytes accessed | tf_op | source)
XLA Modules:
  0.0 43.5 jit_solution(11151000854992240224)
XLA Ops:
  0.6 41.7 %band_backward.1 = (bf16[256,1024]{1,0:T(8,128)(2,1)S(1)}, bf16[256,1024]{1,0:T(8,128)(2,1)S(1)}, bf16[256,1024]{1,0:T(8,128)(2,1)S(1)}, f32[8,320]{1,0:T(8,128)S(1)}) custom-call(bf16[256,1024]{1,0:T(8,128)(2,1)} %q_hbm.1, bf16[256,1024]{1,0:T(8,128)(2,1)} %k_hbm.1, bf16[256,1024]{1,0:T(8,128)(2,1)} %v_hbm.1, bf16[256,1024]{1,0:T(8,128)(2,1)} %g_hbm.1, ...), custom_call_target="tpu_custom_call" | custom-call | tf_op jit(solution)/shard_map/band_backward/pallas_call | solution.py:477
  42.3 1.2 %store.1 = (bf16[256,1024]{1,0:T(8,128)(2,1)}, bf16[256,1024]{1,0:T(8,128)(2,1)}, bf16[256,1024]{1,0:T(8,128)(2,1)}, f32[8,320]{1,0:T(8,128)}) custom-call(bf16[256,1024]{1,0:T(8,128)(2,1)S(1)} %get-tuple-element.8.refs_0_, bf16[256,1024]{1,0:T(8,128)(2,1)S(1)} %get-tuple-element.9.refs_1_, bf16[256,1024]{1,0:T(8,128)(2,1)S(1)} %get-tuple-element.10.refs_2_, ...), custom_call_target="tpu_custom_call" | custom-call | tf_op jit(solution)/shard_map/store/pallas_call | solution.py:519

commit v2 on v1

--- a/solution.py
+++ b/solution.py
@@ -29,6 +29,14 @@
     return stages
 
 
+def flood_reaches(stages):
+    reaches, reach = [], 2
+    while reach < max([stride * (factor - 1) for stride, factor in stages] + [0]):
+        reaches.append(reach)
+        reach *= 2
+    return reaches
+
+
 def iota(shape, axis):
     return lax.broadcasted_iota(jnp.int32, shape, axis)
 
@@ -67,15 +75,15 @@
     sizes,
     q_hbm, k_hbm, v_hbm, g_hbm, log_hbm, dot_hbm, table_hbm,
     dq_ref, dk_ref, dv_ref, dt_ref,
-    q_ref, g_ref, k_ref, v_ref, log_ref, dot_ref, table_ref, load_sem,
+    qg_ref, kv_ref, rows_ref, table_ref, load_sem,
     stat, stat_in, qg_in, part_out, part_in, dq_own, dk_acc, dv_acc,
     bias, edge, tab, neg, const, acc_pos, acc_neg, acc_const, tab_slots,
     stat_send, stat_recv, qg_send, qg_recv, part_send, part_recv, tab_send, tab_recv,
-    qg_load, flood_sem, relay_send,
+    flood_sem, relay_send,
 ):
     sp_size, tp_size = sizes
     total = sp_size * tp_size
-    rows, features = q_ref.shape
+    _, rows, features = qg_ref.shape
     heads, table_len = table_ref.shape
     head_dim = features // heads
     inv_root = head_dim ** -0.5
@@ -90,6 +98,7 @@
 
     group = stages[-1][1] if stages else 1
     inside = lax.rem(me + 1, group) != 0
+    held = min(2, heads)
     sends = [None, (me >= 1) & (lax.rem(me, group) != 0), me >= 2]
     relays = (me + 2 < total) & (lax.rem(me + 2, group) == 0)
 
@@ -103,26 +112,26 @@
     def columns(head):
         return pl.ds(pl.multiple_of(head * head_dim, head_dim), head_dim)
 
-    def qg_load_copy(which, head):
-        return pltpu.make_async_copy(
-            (q_hbm, g_hbm)[which].at[:, columns(head)], (q_ref, g_ref)[which].at[:, columns(head)],
-            qg_load.at[which, head],
-        )
-
-    def start_qg_loads(head):
-        qg_load_copy(0, head).start()
-        qg_load_copy(1, head).start()
-
+    first, others = pl.ds(0, head_dim), pl.ds(head_dim, features - head_dim)
+    stat_rows = (pl.ds(0, heads), pl.ds(heads, heads))
     loads = [
-        pltpu.make_async_copy(source, target, load_sem.at[at])
-        for at, (source, target) in enumerate((
-            (log_hbm, log_ref), (dot_hbm, dot_ref),
-            (table_hbm, table_ref), (k_hbm, k_ref), (v_hbm, v_ref),
-        ))
+        [(q_hbm.at[:, first], qg_ref.at[0, :, first]), (g_hbm.at[:, first], qg_ref.at[1, :, first])],
+        [(log_hbm, rows_ref.at[stat_rows[0]]), (dot_hbm, rows_ref.at[stat_rows[1]])],
+        [(q_hbm.at[:, others], qg_ref.at[0, :, others]), (g_hbm.at[:, others], qg_ref.at[1, :, others])],
+        [(table_hbm, table_ref)],
+        [(k_hbm, kv_ref.at[0]), (v_hbm, kv_ref.at[1])],
     ]
-    start_qg_loads(0)
-    for load in loads[:2]:
-        load.start()
+    loaded = [qg_ref.at[:, :, first], rows_ref, qg_ref.at[:, :, others], table_ref, kv_ref]
+
+    def load_start(at):
+        for source, target in loads[at]:
+            pltpu.make_async_copy(source, target, load_sem.at[at]).start()
+
+    def load_wait(at):
+        pltpu.make_async_copy(loaded[at], loaded[at], load_sem.at[at]).wait()
+
+    load_start(0)
+    load_start(1)
 
     barrier = pltpu.get_barrier_semaphore()
     count = 0
@@ -135,9 +144,8 @@
             def _():
                 pl.semaphore_signal(barrier, inc=1, device_id=device(other), device_id_type=MESH)
 
-    pl.loop(1, heads)(start_qg_loads)
-    for load in loads[2:]:
-        load.start()
+    for at in range(2, len(loads)):
+        load_start(at)
     pl.semaphore_wait(barrier, count)
 
     def stat_copy(lag):
@@ -147,58 +155,58 @@
             device_id=device(me - lag), device_id_type=MESH,
         )
 
-    def qg_copy(lag, which, head):
+    def qg_copy(lag, head):
         return pltpu.make_async_remote_copy(
-            src_ref=(q_ref, g_ref)[which].at[:, columns(head)],
-            dst_ref=qg_in.at[lag - 1, which, head],
-            send_sem=qg_send.at[lag - 1, which, head], recv_sem=qg_recv.at[lag - 1, which, head],
+            src_ref=qg_ref.at[:, :, columns(head)], dst_ref=qg_in.at[lag - 1, head],
+            send_sem=qg_send.at[lag - 1], recv_sem=qg_recv.at[lag - 1, head],
             device_id=device(me - lag), device_id_type=MESH,
         )
 
-    def relay_copy(which, head):
+    def relay_copy(head):
         return pltpu.make_async_remote_copy(
-            src_ref=qg_in.at[1, which, head], dst_ref=qg_in.at[0, which, head],
-            send_sem=relay_send.at[which, head], recv_sem=qg_recv.at[0, which, head],
+            src_ref=qg_in.at[1, head], dst_ref=qg_in.at[0, head],
+            send_sem=relay_send.at[0], recv_sem=qg_recv.at[0, head],
             device_id=device(me + 1), device_id_type=MESH,
         )
 
     def relay(head):
-        for which in (0, 1):
-            qg_copy(2, which, head).wait_recv()
-            relay_copy(which, head).start()
+        qg_copy(2, head).wait_recv()
+        relay_copy(head).start()
 
     def part_copy(lag, head):
         return pltpu.make_async_remote_copy(
             src_ref=part_out.at[lag - 1, head], dst_ref=part_in.at[lag - 1, head],
-            send_sem=part_send.at[lag - 1, head], recv_sem=part_recv.at[lag - 1, head],
+            send_sem=part_send.at[lag - 1],
+            recv_sem=part_recv.at[head if lag == 1 else heads],
             device_id=device(me + lag), device_id_type=MESH,
         )
 
+    def whole(ref, send_sem, recv_sem):
+        return pltpu.make_async_remote_copy(
+            src_ref=ref, dst_ref=ref, send_sem=send_sem, recv_sem=recv_sem,
+            device_id=device(me), device_id_type=MESH,
+        )
+
     def send_qg(head):
-        qg_load_copy(0, head).wait()
-        qg_load_copy(1, head).wait()
         for lag in (1, 2):
             @pl.when(sends[lag])
             def _():
-                qg_copy(lag, 0, head).start()
-                qg_copy(lag, 1, head).start()
-
+                qg_copy(lag, head).start()
+
+    load_wait(0)
     send_qg(0)
-    for load in loads[:2]:
-        load.wait()
-    stat[0:heads, :] = log_ref[...] * LOG2E
-    stat[heads:, :] = dot_ref[...]
+    load_wait(1)
+    stat[0:heads, :] = rows_ref[0:heads, :] * LOG2E
+    stat[heads:, :] = rows_ref[heads:, :]
     for lag in (1, 2):
         @pl.when(me >= lag)
         def _():
             stat_copy(lag).start()
 
+    load_wait(2)
     pl.loop(1, heads)(send_qg)
 
-    reaches, reach = [], 2
-    while reach < max([stride * (factor - 1) for stride, factor in stages] + [0]):
-        reaches.append(reach)
-        reach *= 2
+    reaches = flood_reaches(stages)
 
     def flood_others(at):
         others = (me + reaches[at], me - reaches[at])
@@ -221,7 +229,7 @@
 
     flood_start(0)
 
-    loads[2].wait()
+    load_wait(3)
     tab[...] = jnp.zeros_like(tab)
     tab[:, 0:table_len] = table_ref[...] * LOG2E
     padded = tab[...]
@@ -253,7 +261,7 @@
         bias[0, head] = jnp.where(upper, near, jnp.where(segs_ok, tall, MASKED))
 
     def pair_terms(lag, head, queries, grads, log_row, dot_row):
-        keys, values = k_ref[:, columns(head)], v_ref[:, columns(head)]
+        keys, values = kv_ref[0, :, columns(head)], kv_ref[1, :, columns(head)]
         across = (((1,), (1,)), ((), ()))
         scores = lax.dot_general(keys, queries, across, preferred_element_type=jnp.float32)
         if lag < 2:
@@ -273,14 +281,13 @@
         )
         return score_grads, query_part, key_part, value_part
 
-    loads[3].wait()
-    loads[4].wait()
+    load_wait(4)
     in_loop = min(len(reaches), heads // 2)
 
     @pl.loop(0, heads)
     def _(head):
         score_grads, query_part, key_part, value_part = pair_terms(
-            0, head, q_ref[:, columns(head)], g_ref[:, columns(head)],
+            0, head, qg_ref[0, :, columns(head)], qg_ref[1, :, columns(head)],
             stat[pl.ds(head, 1), :], stat[pl.ds(head + heads, 1), :],
         )
         dq_own[head] = query_part
@@ -294,6 +301,7 @@
         )
         acc_neg[head] = fold_diagonals(tiles)
         acc_const[head] = jnp.zeros(acc_const.shape[1:], jnp.float32)
+
         @pl.when(relays & (lax.rem(head, 2) == 1))
         def _():
             relay(head // 2)
@@ -329,11 +337,10 @@
             def _():
                 @pl.when((lag == 1) | ~relays)
                 def _():
-                    qg_copy(lag, 0, head).wait_recv()
-                    qg_copy(lag, 1, head).wait_recv()
+                    qg_copy(lag, head).wait_recv()
 
                 score_grads, query_part, key_part, value_part = pair_terms(
-                    lag, head, qg_in[lag - 1, 0, head], qg_in[lag - 1, 1, head],
+                    lag, head, qg_in[lag - 1, head, 0], qg_in[lag - 1, head, 1],
                     stat_in[lag - 1, pl.ds(head, 1), :],
                     stat_in[lag - 1, pl.ds(head + heads, 1), :],
                 )
@@ -351,7 +358,7 @@
 
         @pl.when((me + 1 < total) & inside & (head == heads - 2))
         def _():
-            start_parts(0, heads - 1)
+            start_parts(0, heads - held)
 
         dk_ref[:, columns(head)] = (dk_acc[head] * inv_root).astype(dk_ref.dtype)
         dv_ref[:, columns(head)] = dv_acc[head].astype(dv_ref.dtype)
@@ -373,7 +380,7 @@
         stage = stages[at]
         return pltpu.make_async_remote_copy(
             src_ref=tab_slots.at[at, place], dst_ref=tab_slots.at[at, place],
-            send_sem=tab_send.at[at, peer_place], recv_sem=tab_recv.at[at, place],
+            send_sem=tab_send.at[at], recv_sem=tab_recv.at[at],
             device_id=stage_peer(stage, peer_place), device_id_type=MESH,
         )
 
@@ -385,40 +392,44 @@
 
     def stage_finish(at):
         factor = stages[at][1]
-        place = stage_place(stages[at])
-        for offset in range(1, factor):
-            other = lax.rem(place + offset, factor)
-            tab_copy(at, other, other).wait_recv()
+        peers = tab_slots.at[at, pl.ds(0, factor - 1)]
+        whole(peers, tab_send.at[at], tab_recv.at[at]).wait_recv()
         out = tab_slots[at, 0]
         for member in range(1, factor):
             out = out + tab_slots[at, member]
         return out
 
-    def finish_queries(first, last):
-        @pl.loop(first, last)
-        def _(head):
-            for lag in (2, 1):
-                @pl.when(me >= lag)
-                def _():
-                    part_copy(lag, head).wait_recv()
-                    dq_own[head] += part_in[lag - 1, head].astype(jnp.float32)
-            dq_ref[:, columns(head)] = (dq_own[head] * inv_root).astype(dq_ref.dtype)
-
     if stages:
         stage_start(0, running)
 
     @pl.when((me + 1 < total) & ~inside)
     def _():
-        start_parts(0, heads)
+        start_parts(0, heads - held)
 
     for at in range(len(stages) - 1):
         stage_start(at + 1, stage_finish(at))
 
-    @pl.when((me + 1 < total) & inside)
+    @pl.when(me + 1 < total)
     def _():
-        start_parts(heads - 1, heads)
-
-    finish_queries(0, heads)
+        start_parts(heads - held, heads)
+
+    @pl.when(me >= 2)
+    def _():
+        whole(part_in.at[1], part_send.at[1], part_recv.at[heads]).wait_recv()
+
+        @pl.loop(0, heads)
+        def _(head):
+            dq_own[head] += part_in[1, head].astype(jnp.float32)
+
+    @pl.loop(0, heads)
+    def _(head):
+        @pl.when(me >= 1)
+        def _():
+            part_copy(1, head).wait_recv()
+            dq_own[head] += part_in[0, head].astype(jnp.float32)
+
+        dq_ref[:, columns(head)] = (dq_own[head] * inv_root).astype(dq_ref.dtype)
+
     if stages:
         running = stage_finish(len(stages) - 1)
     dt_ref[...] = running[:, 0:table_len]
@@ -428,27 +439,21 @@
         def _():
             stat_copy(lag).wait_send()
 
-    @pl.loop(0, heads)
-    def _(head):
-        for lag in (1, 2):
-            @pl.when(sends[lag])
-            def _():
-                qg_copy(lag, 0, head).wait_send()
-                qg_copy(lag, 1, head).wait_send()
-
-            @pl.when(me + lag < total)
-            def _():
-                part_copy(lag, head).wait_send()
-
-        @pl.when(relays)
-        def _():
-            relay_copy(0, head).wait_send()
-            relay_copy(1, head).wait_send()
-
-    for at, stage in enumerate(stages):
-        place = stage_place(stage)
-        for offset in range(1, stage[1]):
-            tab_copy(at, place, lax.rem(place + offset, stage[1])).wait_send()
+        @pl.when(sends[lag])
+        def _():
+            whole(qg_ref, qg_send.at[lag - 1], qg_recv.at[lag - 1, 0]).wait_send()
+
+        @pl.when(me + lag < total)
+        def _():
+            whole(part_out.at[lag - 1], part_send.at[lag - 1], part_recv.at[0]).wait_send()
+
+    @pl.when(relays)
+    def _():
+        whole(qg_in.at[1], relay_send.at[0], qg_recv.at[0, 0]).wait_send()
+
+    for at, (_, factor) in enumerate(stages):
+        peers = tab_slots.at[at, pl.ds(0, factor - 1)]
+        whole(peers, tab_send.at[at], tab_recv.at[at]).wait_send()
 
 
 def store_kernel(*refs):
@@ -468,6 +473,7 @@
     assert table_len == REL_CLIP + SEG_LEN and head_dim == LANES
     stage_list = axis_stages(sizes[0] * sizes[1])
     stage_count = max(len(stage_list), 1)
+    flood_count = max(len(flood_reaches(stage_list)), 1)
     slot_count = max([factor for _, factor in stage_list] + [1])
     table_width = -(-(table_len + 1) // LANES) * LANES
     f32, bf16 = jnp.float32, jnp.bfloat16
@@ -480,17 +486,14 @@
         in_specs=[pl.BlockSpec(memory_space=pltpu.HBM)] * 7,
         out_specs=(vmem,) * 4,
         scratch_shapes=[
-            pltpu.VMEM((rows, features), bf16),
-            pltpu.VMEM((rows, features), bf16),
-            pltpu.VMEM((rows, features), bf16),
-            pltpu.VMEM((rows, features), bf16),
-            pltpu.VMEM((heads, rows), f32),
-            pltpu.VMEM((heads, rows), f32),
+            pltpu.VMEM((2, rows, features), bf16),
+            pltpu.VMEM((2, rows, features), bf16),
+            pltpu.VMEM((2 * heads, rows), f32),
             pltpu.VMEM((heads, table_len), f32),
             dma((5,)),
             pltpu.VMEM((2 * heads, rows), f32),
             pltpu.VMEM((2, 2 * heads, rows), f32),
-            pltpu.VMEM((2, 2, heads, rows, head_dim), bf16),
+            pltpu.VMEM((2, heads, 2, rows, head_dim), bf16),
             pltpu.VMEM((2, heads, rows, head_dim), bf16),
             pltpu.VMEM((2, heads, rows, head_dim), bf16),
             pltpu.VMEM((heads, rows, head_dim), f32),
@@ -506,10 +509,10 @@
             pltpu.VMEM((heads, SUBL, rows), f32),
             pltpu.VMEM((stage_count, slot_count, heads, table_width), f32),
             dma((2,)), dma((2,)),
-            dma((2, 2, heads)), dma((2, 2, heads)),
-            dma((2, heads)), dma((2, heads)),
-            dma((stage_count, slot_count)), dma((stage_count, slot_count)),
-            dma((2, heads)), pltpu.SemaphoreType.REGULAR((16,)), dma((2, heads)),
+            dma((2,)), dma((2, heads)),
+            dma((2,)), dma((heads + 1,)),
+            dma((stage_count,)), dma((stage_count,)),
+            pltpu.SemaphoreType.REGULAR((flood_count,)), dma((1,)),
         ],
         compiler_params=pltpu.CompilerParams(
             collective_id=0, has_side_effects=True, vmem_limit_bytes=40 * 2**20

time: 43.6 us -> 41.2 us (0.945)
  Pallas kernels: 42.8 us -> 40.1 us
    pallas_call x1, Pallas kernels: 41.7 us -> 38.9 us  [local(): pl.pallas_call(functools.partial(kernel, sizes), out_shape=(wide, wide, w...]
where the time goes in v2:
time: 41.2 us; the launch traced here: 40.7 us
  Pallas kernels  40.1 us (97%)
  between operations  0.64 us (2%)
    pallas_call x1, Pallas kernels, local(): pl.pallas_call(functools.partial(kernel, sizes), out_shape=(wide, wide, w...  38.9 us
    pallas_call x1, Pallas kernels, local(): pl.pallas_call(store_kernel, out_shape=tuple((jax.ShapeDtypeStruct(x.shap...  1.18 us

profile of v2, /device:TPU:0, one launch (start us, length us, event | category | flops | bytes accessed | tf_op | source)
XLA Modules:
  0.0 40.7 jit_solution(7604382252871022028)
XLA Ops:
  0.6 38.9 %band_backward.1 = (bf16[256,1024]{1,0:T(8,128)(2,1)S(1)}, bf16[256,1024]{1,0:T(8,128)(2,1)S(1)}, bf16[256,1024]{1,0:T(8,128)(2,1)S(1)}, f32[8,320]{1,0:T(8,128)S(1)}) custom-call(bf16[256,1024]{1,0:T(8,128)(2,1)} %q_hbm.1, bf16[256,1024]{1,0:T(8,128)(2,1)} %k_hbm.1, bf16[256,1024]{1,0:T(8,128)(2,1)} %v_hbm.1, bf16[256,1024]{1,0:T(8,128)(2,1)} %g_hbm.1, ...), custom_call_target="tpu_custom_call" | custom-call | tf_op jit(solution)/shard_map/band_backward/pallas_call | solution.py:483
  39.5 1.2 %store.1 = (bf16[256,1024]{1,0:T(8,128)(2,1)}, bf16[256,1024]{1,0:T(8,128)(2,1)}, bf16[256,1024]{1,0:T(8,128)(2,1)}, f32[8,320]{1,0:T(8,128)}) custom-call(bf16[256,1024]{1,0:T(8,128)(2,1)S(1)} %get-tuple-element.8.refs_0_, bf16[256,1024]{1,0:T(8,128)(2,1)S(1)} %get-tuple-element.9.refs_1_, bf16[256,1024]{1,0:T(8,128)(2,1)S(1)} %get-tuple-element.10.refs_2_, ...), custom_call_target="tpu_custom_call" | custom-call | tf_op jit(solution)/shard_map/store/pallas_call | solution.py:522

commit v3 on v2

--- a/solution.py
+++ b/solution.py
@@ -79,7 +79,7 @@
     stat, stat_in, qg_in, part_out, part_in, dq_own, dk_acc, dv_acc,
     bias, edge, tab, neg, const, acc_pos, acc_neg, acc_const, tab_slots,
     stat_send, stat_recv, qg_send, qg_recv, part_send, part_recv, tab_send, tab_recv,
-    flood_sem, relay_send,
+    flood_sem, go_sem, relay_send,
 ):
     sp_size, tp_size = sizes
     total = sp_size * tp_size
@@ -97,8 +97,7 @@
     stages = axis_stages(total)[::-1]
 
     group = stages[-1][1] if stages else 1
-    inside = lax.rem(me + 1, group) != 0
-    held = min(2, heads)
+    inside = (lax.rem(me + 1, group) != 0) | (lax.rem((me + 1) // group, 2) == 1)
     sends = [None, (me >= 1) & (lax.rem(me, group) != 0), me >= 2]
     relays = (me + 2 < total) & (lax.rem(me + 2, group) == 0)
 
@@ -130,21 +129,23 @@
     def load_wait(at):
         pltpu.make_async_copy(loaded[at], loaded[at], load_sem.at[at]).wait()
 
-    load_start(0)
-    load_start(1)
-
+    place = lax.rem(me, group)
+    odd_group = lax.rem(me // group, 2) == 1
+    held = jnp.where(place == 0, 1, jnp.where(place == 1, jnp.where(odd_group, 1, 3), jnp.where(place == 2, 1, 2)))
     barrier = pltpu.get_barrier_semaphore()
-    count = 0
-    for lag in (1, 2):
-        for other in (me + lag, me - lag):
-            valid = (other >= 0) & (other < total)
-            count = count + jnp.where(valid, 1, 0)
-
-            @pl.when(valid)
-            def _():
-                pl.semaphore_signal(barrier, inc=1, device_id=device(other), device_id_type=MESH)
-
-    for at in range(2, len(loads)):
+    for other, valid in (
+        (me + 2, (me + 2 < total) & (place != group - 1)),
+        (me + 1, me + 1 < total),
+        (me - 1, lax.rem(place, 2) == 1),
+    ):
+        @pl.when(valid)
+        def _():
+            pl.semaphore_signal(barrier, inc=1, device_id=device(other), device_id_type=MESH)
+
+    awaited = (me >= 1, (me >= 2) & (place != 1), (lax.rem(place, 2) == 0) & (me + 1 < total))
+    count = sum(jnp.where(valid, 1, 0) for valid in awaited)
+
+    for at in range(len(loads)):
         load_start(at)
     pl.semaphore_wait(barrier, count)
 
@@ -187,24 +188,60 @@
             device_id=device(me), device_id_type=MESH,
         )
 
-    def send_qg(head):
-        for lag in (1, 2):
-            @pl.when(sends[lag])
-            def _():
-                qg_copy(lag, head).start()
-
-    load_wait(0)
-    send_qg(0)
+    for which, source in enumerate((q_hbm, g_hbm)):
+        @pl.when(sends[1])
+        def _():
+            pltpu.make_async_remote_copy(
+                src_ref=source.at[:, first], dst_ref=qg_in.at[0, 0, which],
+                send_sem=qg_send.at[0], recv_sem=qg_recv.at[0, 0],
+                device_id=device(me - 1), device_id_type=MESH,
+            ).start()
+
+    @pl.when((place == 0) & (me >= 1))
+    def _():
+        pl.semaphore_signal(go_sem.at[0], inc=1, device_id=device(me + 1), device_id_type=MESH)
+
+    @pl.when(sends[2] & (place != 1))
+    def _():
+        load_wait(0)
+        qg_copy(2, 0).start()
+
+    @pl.when(~(sends[2] & (place != 1)))
+    def _():
+        load_wait(0)
+
     load_wait(1)
     stat[0:heads, :] = rows_ref[0:heads, :] * LOG2E
     stat[heads:, :] = rows_ref[heads:, :]
-    for lag in (1, 2):
-        @pl.when(me >= lag)
-        def _():
-            stat_copy(lag).start()
+
+    @pl.when(me >= 1)
+    def _():
+        stat_copy(1).start()
 
     load_wait(2)
-    pl.loop(1, heads)(send_qg)
+
+    @pl.loop(1, heads)
+    def _(head):
+        @pl.when(sends[1])
+        def _():
+            qg_copy(1, head).start()
+
+        @pl.when(sends[2] & (place != 1))
+        def _():
+            qg_copy(2, head).start()
+
+    @pl.when(sends[2])
+    def _():
+        @pl.when(place == 1)
+        def _():
+            pl.semaphore_wait(go_sem.at[0], 1)
+
+            @pl.loop(0, heads)
+            def _(head):
+                qg_copy(2, head).start()
+
+        stat_copy(2).start()
+        pl.semaphore_signal(flood_sem.at[0], inc=1, device_id=device(me - 2), device_id_type=MESH)
 
     reaches = flood_reaches(stages)
 
@@ -218,16 +255,18 @@
                 @pl.when(valid)
                 def _():
                     pl.semaphore_signal(
-                        flood_sem.at[at], inc=1, device_id=device(other), device_id_type=MESH
+                        flood_sem.at[at + 1], inc=1, device_id=device(other), device_id_type=MESH
                     )
 
     def flood_finish(at):
         if at < len(reaches):
-            pl.semaphore_wait(
-                flood_sem.at[at], sum(jnp.where(valid, 1, 0) for _, valid in flood_others(at))
-            )
-
-    flood_start(0)
+            valid = [valid for _, valid in flood_others(at)]
+
+            @pl.when(valid[0] | valid[1])
+            def _():
+                pl.semaphore_wait(
+                    flood_sem.at[at + 1], sum(jnp.where(each, 1, 0) for each in valid)
+                )
 
     load_wait(3)
     tab[...] = jnp.zeros_like(tab)
@@ -282,7 +321,18 @@
         return score_grads, query_part, key_part, value_part
 
     load_wait(4)
-    in_loop = min(len(reaches), heads // 2)
+    steps = len(reaches) + 1 if stages else 0
+    in_loop = min(steps, heads // 2)
+
+    def flood_step(at):
+        if at == 0:
+            @pl.when(me + 2 < total)
+            def _():
+                pl.semaphore_wait(flood_sem.at[0], 1)
+        else:
+            flood_finish(at - 1)
+        flood_start(at)
+
 
     @pl.loop(0, heads)
     def _(head):
@@ -309,17 +359,15 @@
         for at in range(in_loop):
             @pl.when(head == 2 * at + 1)
             def _():
-                flood_finish(at)
-                flood_start(at + 1)
+                flood_step(at)
 
     def start_parts(first, last):
         @pl.loop(first, last)
         def _(head):
             part_copy(1, head).start()
 
-    for at in range(in_loop, len(reaches)):
-        flood_finish(at)
-        flood_start(at + 1)
+    for at in range(in_loop, steps):
+        flood_step(at)
 
     for lag in (2, 1):
         @pl.when(me + lag < total)
@@ -473,7 +521,8 @@
     assert table_len == REL_CLIP + SEG_LEN and head_dim == LANES
     stage_list = axis_stages(sizes[0] * sizes[1])
     stage_count = max(len(stage_list), 1)
-    flood_count = max(len(flood_reaches(stage_list)), 1)
+    flood_count = len(flood_reaches(stage_list)) + 1
+    assert sizes[0] * sizes[1] % 4 == 0
     slot_count = max([factor for _, factor in stage_list] + [1])
     table_width = -(-(table_len + 1) // LANES) * LANES
     f32, bf16 = jnp.float32, jnp.bfloat16
@@ -512,7 +561,8 @@
             dma((2,)), dma((2, heads)),
             dma((2,)), dma((heads + 1,)),
             dma((stage_count,)), dma((stage_count,)),
-            pltpu.SemaphoreType.REGULAR((flood_count,)), dma((1,)),
+            pltpu.SemaphoreType.REGULAR((flood_count,)),
+            pltpu.SemaphoreType.REGULAR((1,)), dma((1,)),
         ],
         compiler_params=pltpu.CompilerParams(
             collective_id=0, has_side_effects=True, vmem_limit_bytes=40 * 2**20

time: 41.2 us -> 40.7 us (0.988)
  Pallas kernels: 40.1 us -> 39.5 us
    pallas_call x1, Pallas kernels: 38.9 us -> 38.3 us  [local(): pl.pallas_call(functools.partial(kernel, sizes), out_shape=(wide, wide, w...]
where the time goes in v3:
time: 40.7 us; the launch traced here: 40.1 us
  Pallas kernels  39.5 us (97%)
  between operations  0.64 us (2%)
    pallas_call x1, Pallas kernels, local(): pl.pallas_call(functools.partial(kernel, sizes), out_shape=(wide, wide, w...  38.3 us
    pallas_call x1, Pallas kernels, local(): pl.pallas_call(store_kernel, out_shape=tuple((jax.ShapeDtypeStruct(x.shap...  1.18 us

profile of v3, /device:TPU:0, one launch (start us, length us, event | category | flops | bytes accessed | tf_op | source)
XLA Modules:
  0.0 40.1 jit_solution(2440560293835376780)
XLA Ops:
  0.6 38.3 %band_backward.1 = (bf16[256,1024]{1,0:T(8,128)(2,1)S(1)}, bf16[256,1024]{1,0:T(8,128)(2,1)S(1)}, bf16[256,1024]{1,0:T(8,128)(2,1)S(1)}, f32[8,320]{1,0:T(8,128)S(1)}) custom-call(bf16[256,1024]{1,0:T(8,128)(2,1)} %q_hbm.1, bf16[256,1024]{1,0:T(8,128)(2,1)} %k_hbm.1, bf16[256,1024]{1,0:T(8,128)(2,1)} %v_hbm.1, bf16[256,1024]{1,0:T(8,128)(2,1)} %g_hbm.1, ...), custom_call_target="tpu_custom_call" | custom-call | tf_op jit(solution)/shard_map/band_backward/pallas_call | solution.py:532
  38.9 1.2 %store.1 = (bf16[256,1024]{1,0:T(8,128)(2,1)}, bf16[256,1024]{1,0:T(8,128)(2,1)}, bf16[256,1024]{1,0:T(8,128)(2,1)}, f32[8,320]{1,0:T(8,128)}) custom-call(bf16[256,1024]{1,0:T(8,128)(2,1)S(1)} %get-tuple-element.8.refs_0_, bf16[256,1024]{1,0:T(8,128)(2,1)S(1)} %get-tuple-element.9.refs_1_, bf16[256,1024]{1,0:T(8,128)(2,1)S(1)} %get-tuple-element.10.refs_2_, ...), custom_call_target="tpu_custom_call" | custom-call | tf_op jit(solution)/shard_map/store/pallas_call | solution.py:572

commit v4 on v3

--- a/solution.py
+++ b/solution.py
@@ -130,8 +130,7 @@
         pltpu.make_async_copy(loaded[at], loaded[at], load_sem.at[at]).wait()
 
     place = lax.rem(me, group)
-    odd_group = lax.rem(me // group, 2) == 1
-    held = jnp.where(place == 0, 1, jnp.where(place == 1, jnp.where(odd_group, 1, 3), jnp.where(place == 2, 1, 2)))
+    held = min(2, heads)
     barrier = pltpu.get_barrier_semaphore()
     for other, valid in (
         (me + 2, (me + 2 < total) & (place != group - 1)),
@@ -218,6 +217,10 @@
     def _():
         stat_copy(1).start()
 
+    @pl.when(sends[2] & (place != 1))
+    def _():
+        stat_copy(2).start()
+
     load_wait(2)
 
     @pl.loop(1, heads)
@@ -235,12 +238,12 @@
         @pl.when(place == 1)
         def _():
             pl.semaphore_wait(go_sem.at[0], 1)
+            stat_copy(2).start()
 
             @pl.loop(0, heads)
             def _(head):
                 qg_copy(2, head).start()
 
-        stat_copy(2).start()
         pl.semaphore_signal(flood_sem.at[0], inc=1, device_id=device(me - 2), device_id_type=MESH)
 
     reaches = flood_reaches(stages)

time: 40.7 us -> 40.8 us (level)
  Pallas kernels: 39.5 us -> 40 us
    pallas_call x1, Pallas kernels: 38.3 us -> 38.8 us  [local(): pl.pallas_call(functools.partial(kernel, sizes), out_shape=(wide, wide, w...]
where the time goes in v4:
time: 40.8 us; the launch traced here: 40.6 us
  Pallas kernels  40 us (98%)
  between operations  0.64 us (2%)
    pallas_call x1, Pallas kernels, local(): pl.pallas_call(functools.partial(kernel, sizes), out_shape=(wide, wide, w...  38.8 us
    pallas_call x1, Pallas kernels, local(): pl.pallas_call(store_kernel, out_shape=tuple((jax.ShapeDtypeStruct(x.shap...  1.18 us

profile of v4, /device:TPU:0, one launch (start us, length us, event | category | flops | bytes accessed | tf_op | source)
XLA Modules:
  0.0 40.6 jit_solution(3451702895989286584)
XLA Ops:
  0.6 38.8 %band_backward.1 = (bf16[256,1024]{1,0:T(8,128)(2,1)S(1)}, bf16[256,1024]{1,0:T(8,128)(2,1)S(1)}, bf16[256,1024]{1,0:T(8,128)(2,1)S(1)}, f32[8,320]{1,0:T(8,128)S(1)}) custom-call(bf16[256,1024]{1,0:T(8,128)(2,1)} %q_hbm.1, bf16[256,1024]{1,0:T(8,128)(2,1)} %k_hbm.1, bf16[256,1024]{1,0:T(8,128)(2,1)} %v_hbm.1, bf16[256,1024]{1,0:T(8,128)(2,1)} %g_hbm.1, ...), custom_call_target="tpu_custom_call" | custom-call | tf_op jit(solution)/shard_map/band_backward/pallas_call | solution.py:535
  39.4 1.2 %store.1 = (bf16[256,1024]{1,0:T(8,128)(2,1)}, bf16[256,1024]{1,0:T(8,128)(2,1)}, bf16[256,1024]{1,0:T(8,128)(2,1)}, f32[8,320]{1,0:T(8,128)}) custom-call(bf16[256,1024]{1,0:T(8,128)(2,1)S(1)} %get-tuple-element.8.refs_0_, bf16[256,1024]{1,0:T(8,128)(2,1)S(1)} %get-tuple-element.9.refs_1_, bf16[256,1024]{1,0:T(8,128)(2,1)S(1)} %get-tuple-element.10.refs_2_, ...), custom_call_target="tpu_custom_call" | custom-call | tf_op jit(solution)/shard_map/store/pallas_call | solution.py:575

commit v5 on v4

--- a/solution.py
+++ b/solution.py
@@ -79,7 +79,7 @@
     stat, stat_in, qg_in, part_out, part_in, dq_own, dk_acc, dv_acc,
     bias, edge, tab, neg, const, acc_pos, acc_neg, acc_const, tab_slots,
     stat_send, stat_recv, qg_send, qg_recv, part_send, part_recv, tab_send, tab_recv,
-    flood_sem, go_sem, relay_send,
+    flood_sem, go_sem, relay_send, detour_in, detour_send, detour_recv,
 ):
     sp_size, tp_size = sizes
     total = sp_size * tp_size
@@ -130,7 +130,7 @@
         pltpu.make_async_copy(loaded[at], loaded[at], load_sem.at[at]).wait()
 
     place = lax.rem(me, group)
-    held = min(2, heads)
+    held = jnp.where(place == 0, 1, jnp.where(place == 1, jnp.where(lax.rem(me // group, 2) == 1, 1, 2), 2))
     barrier = pltpu.get_barrier_semaphore()
     for other, valid in (
         (me + 2, (me + 2 < total) & (place != group - 1)),
@@ -364,10 +364,36 @@
             def _():
                 flood_step(at)
 
+    detours = heads // 2
+    leaves = (place == group - 1) & (me // group == 0) & (me + 2 < total)
+    passes = (place == 1) & (me // group == 1)
+
+    def leave_copy(head):
+        return pltpu.make_async_remote_copy(
+            src_ref=part_out.at[0, head], dst_ref=detour_in.at[head],
+            send_sem=part_send.at[0], recv_sem=detour_recv.at[0],
+            device_id=device(me + 2), device_id_type=MESH,
+        )
+
+    def pass_copy(head):
+        return pltpu.make_async_remote_copy(
+            src_ref=detour_in.at[head], dst_ref=part_in.at[0, head],
+            send_sem=detour_send.at[0], recv_sem=part_recv.at[head],
+            device_id=device(me - 1), device_id_type=MESH,
+        )
+
     def start_parts(first, last):
         @pl.loop(first, last)
         def _(head):
-            part_copy(1, head).start()
+            detour = leaves & (head < detours)
+
+            @pl.when(detour)
+            def _():
+                leave_copy(head).start()
+
+            @pl.when(~detour)
+            def _():
+                part_copy(1, head).start()
 
     for at in range(in_loop, steps):
         flood_step(at)
@@ -464,6 +490,14 @@
     def _():
         start_parts(heads - held, heads)
 
+    @pl.when(passes)
+    def _():
+        whole(detour_in, detour_send.at[0], detour_recv.at[0]).wait_recv()
+
+        @pl.loop(0, detours)
+        def _(head):
+            pass_copy(head).start()
+
     @pl.when(me >= 2)
     def _():
         whole(part_in.at[1], part_send.at[1], part_recv.at[heads]).wait_recv()
@@ -501,6 +535,10 @@
     @pl.when(relays)
     def _():
         whole(qg_in.at[1], relay_send.at[0], qg_recv.at[0, 0]).wait_send()
+
+    @pl.when(passes)
+    def _():
+        whole(detour_in, detour_send.at[0], detour_recv.at[0]).wait_send()
 
     for at, (_, factor) in enumerate(stages):
         peers = tab_slots.at[at, pl.ds(0, factor - 1)]
@@ -566,6 +604,7 @@
             dma((stage_count,)), dma((stage_count,)),
             pltpu.SemaphoreType.REGULAR((flood_count,)),
             pltpu.SemaphoreType.REGULAR((1,)), dma((1,)),
+            pltpu.VMEM((heads // 2, rows, head_dim), bf16), dma((1,)), dma((1,)),
         ],
         compiler_params=pltpu.CompilerParams(
             collective_id=0, has_side_effects=True, vmem_limit_bytes=40 * 2**20

time: 40.8 us -> 40.8 us (level)
  no operation moved by 1% of the time
where the time goes in v5:
time: 40.8 us; the launch traced here: 40.6 us
  Pallas kernels  40 us (98%)
  between operations  0.64 us (2%)
    pallas_call x1, Pallas kernels, local(): pl.pallas_call(functools.partial(kernel, sizes), out_shape=(wide, wide, w...  38.8 us
    pallas_call x1, Pallas kernels, local(): pl.pallas_call(store_kernel, out_shape=tuple((jax.ShapeDtypeStruct(x.shap...  1.18 us

profile of v5, /device:TPU:0, one launch (start us, length us, event | category | flops | bytes accessed | tf_op | source)
XLA Modules:
  0.0 40.6 jit_solution(13439446245799512700)
XLA Ops:
  0.6 38.8 %band_backward.1 = (bf16[256,1024]{1,0:T(8,128)(2,1)S(1)}, bf16[256,1024]{1,0:T(8,128)(2,1)S(1)}, bf16[256,1024]{1,0:T(8,128)(2,1)S(1)}, f32[8,320]{1,0:T(8,128)S(1)}) custom-call(bf16[256,1024]{1,0:T(8,128)(2,1)} %q_hbm.1, bf16[256,1024]{1,0:T(8,128)(2,1)} %k_hbm.1, bf16[256,1024]{1,0:T(8,128)(2,1)} %v_hbm.1, bf16[256,1024]{1,0:T(8,128)(2,1)} %g_hbm.1, ...), custom_call_target="tpu_custom_call" | custom-call | tf_op jit(solution)/shard_map/band_backward/pallas_call | solution.py:573
  39.4 1.2 %store.1 = (bf16[256,1024]{1,0:T(8,128)(2,1)}, bf16[256,1024]{1,0:T(8,128)(2,1)}, bf16[256,1024]{1,0:T(8,128)(2,1)}, f32[8,320]{1,0:T(8,128)}) custom-call(bf16[256,1024]{1,0:T(8,128)(2,1)S(1)} %get-tuple-element.8.refs_0_, bf16[256,1024]{1,0:T(8,128)(2,1)S(1)} %get-tuple-element.9.refs_1_, bf16[256,1024]{1,0:T(8,128)(2,1)S(1)} %get-tuple-element.10.refs_2_, ...), custom_call_target="tpu_custom_call" | custom-call | tf_op jit(solution)/shard_map/store/pallas_call | solution.py:614

commit v6 on v4

--- a/solution.py
+++ b/solution.py
@@ -177,7 +177,7 @@
         return pltpu.make_async_remote_copy(
             src_ref=part_out.at[lag - 1, head], dst_ref=part_in.at[lag - 1, head],
             send_sem=part_send.at[lag - 1],
-            recv_sem=part_recv.at[head if lag == 1 else heads],
+            recv_sem=part_recv.at[jnp.maximum(head - (heads - held), -1) + 2 if lag == 1 else 0],
             device_id=device(me + lag), device_id_type=MESH,
         )
 
@@ -466,17 +466,25 @@
 
     @pl.when(me >= 2)
     def _():
-        whole(part_in.at[1], part_send.at[1], part_recv.at[heads]).wait_recv()
+        whole(part_in.at[1], part_send.at[1], part_recv.at[0]).wait_recv()
 
         @pl.loop(0, heads)
         def _(head):
             dq_own[head] += part_in[1, head].astype(jnp.float32)
 
+    @pl.when(me >= 1)
+    def _():
+        early = part_in.at[0, pl.ds(0, heads - held)]
+        whole(early, part_send.at[0], part_recv.at[1]).wait_recv()
+
     @pl.loop(0, heads)
     def _(head):
         @pl.when(me >= 1)
         def _():
-            part_copy(1, head).wait_recv()
+            @pl.when(head >= heads - held)
+            def _():
+                part_copy(1, head).wait_recv()
+
             dq_own[head] += part_in[0, head].astype(jnp.float32)
 
         dq_ref[:, columns(head)] = (dq_own[head] * inv_root).astype(dq_ref.dtype)
@@ -562,7 +570,7 @@
             pltpu.VMEM((stage_count, slot_count, heads, table_width), f32),
             dma((2,)), dma((2,)),
             dma((2,)), dma((2, heads)),
-            dma((2,)), dma((heads + 1,)),
+            dma((2,)), dma((4,)),
             dma((stage_count,)), dma((stage_count,)),
             pltpu.SemaphoreType.REGULAR((flood_count,)),
             pltpu.SemaphoreType.REGULAR((1,)), dma((1,)),

time: 40.8 us -> 40.7 us (level)
  no operation moved by 1% of the time
where the time goes in v6:
time: 40.7 us; the launch traced here: 40.6 us
  Pallas kernels  39.9 us (98%)
  between operations  0.64 us (2%)
    pallas_call x1, Pallas kernels, local(): pl.pallas_call(functools.partial(kernel, sizes), out_shape=(wide, wide, w...  38.7 us
    pallas_call x1, Pallas kernels, local(): pl.pallas_call(store_kernel, out_shape=tuple((jax.ShapeDtypeStruct(x.shap...  1.18 us

profile of v6, /device:TPU:0, one launch (start us, length us, event | category | flops | bytes accessed | tf_op | source)
XLA Modules:
  0.0 40.6 jit_solution(17680781910329539348)
XLA Ops:
  0.6 38.7 %band_backward.1 = (bf16[256,1024]{1,0:T(8,128)(2,1)S(1)}, bf16[256,1024]{1,0:T(8,128)(2,1)S(1)}, bf16[256,1024]{1,0:T(8,128)(2,1)S(1)}, f32[8,320]{1,0:T(8,128)S(1)}) custom-call(bf16[256,1024]{1,0:T(8,128)(2,1)} %q_hbm.1, bf16[256,1024]{1,0:T(8,128)(2,1)} %k_hbm.1, bf16[256,1024]{1,0:T(8,128)(2,1)} %v_hbm.1, bf16[256,1024]{1,0:T(8,128)(2,1)} %g_hbm.1, ...), custom_call_target="tpu_custom_call" | custom-call | tf_op jit(solution)/shard_map/band_backward/pallas_call | solution.py:543
  39.4 1.2 %store.1 = (bf16[256,1024]{1,0:T(8,128)(2,1)}, bf16[256,1024]{1,0:T(8,128)(2,1)}, bf16[256,1024]{1,0:T(8,128)(2,1)}, f32[8,320]{1,0:T(8,128)}) custom-call(bf16[256,1024]{1,0:T(8,128)(2,1)S(1)} %get-tuple-element.8.refs_0_, bf16[256,1024]{1,0:T(8,128)(2,1)S(1)} %get-tuple-element.9.refs_1_, bf16[256,1024]{1,0:T(8,128)(2,1)S(1)} %get-tuple-element.10.refs_2_, ...), custom_call_target="tpu_custom_call" | custom-call | tf_op jit(solution)/shard_map/store/pallas_call | solution.py:583
